TPU v7x, 512 devices: a whole 4x4x16 slice. The times are simulated.
512 devices in a mesh: sp: 128 (over z, x, core), tp: 4 (over y).
Axes of the slice: x: 4, y: 4, z: 16, core: 2. Of those that a mesh axis runs over, the one named last changes fastest.
Arguments:
- tokens: bfloat16 [65536, 2048], P('sp', 'tp'), may hold values from -6 to 6
- norm_gain: float32 [2048], replicated, may hold values from 0.1 to 1.9
- w_query: bfloat16 [2048, 1024], P('sp', 'tp'), may hold values from -1 to 1
- w_key: bfloat16 [2048, 256], P('sp', 'tp'), may hold values from -16 to 16
- w_value: bfloat16 [2048, 256], P('sp', 'tp'), may hold values from -1 to 1
- w_post_gate: bfloat16 [2048, 1024], P('sp', 'tp'), may hold values from -0.125 to 0.125
- w_pre_gate: bfloat16 [2048, 1024], P('sp', 'tp'), may hold values from -0.125 to 0.125
- w_conv_in: bfloat16 [2048, 1024], P('sp', 'tp'), may hold values from -0.125 to 0.125
- conv_taps: float32 [3, 1024], P(None, 'tp'), may hold values from -3 to 3
- sink_logit: float32 [16], P('tp'), may hold values from 2 to 6
- w_out_attn: bfloat16 [1024, 2048], P('tp', 'sp'), may hold values from -0.1875 to 0.1875
- w_out_conv: bfloat16 [1024, 2048], P('tp', 'sp'), may hold values from -0.1875 to 0.1875
Outputs:
- mixed: bfloat16 [65536, 2048], P(('sp', 'tp'))
- log_weight_sum: float32 [16, 65536], P('tp', 'sp')
All inputs are finite; a program needn't handle non-finite values.
Results may differ from a plain program's by a relative error of at most 0.012.
The roundings to bfloat16 on the way count: a program that leaves them out, or rounds other values in their place, can miss the bound.
Values may be sent and summed in bfloat16 or wider, within the bound.
No kernel may reach another device: no remote copies, remote signals or barrier semaphores. Data moves between devices by JAX's collectives and lax.ppermute only.
A program may use at most 64 MiB of HBM per device.

v0:
```python
import functools

import jax
import jax.numpy as jnp
from jax import lax
from jax.experimental import pallas as pl
from jax.experimental.pallas import tpu as pltpu
from jax.sharding import Mesh
from jax.sharding import PartitionSpec as P


HEAD_DIM = 64
WINDOW = 128
GRID_W = 64
TOKENS = 65536
SP = ("sp_0", "sp_1", "sp_2")
SP_TP = (*SP, "tp")


rope_base = 10000.0
norm_eps = 1e-06


Z, X, CORE = "sp_0", "sp_1", "sp_2"
VMEM = pl.BlockSpec(memory_space=pltpu.VMEM)
SMEM = pl.BlockSpec(memory_space=pltpu.SMEM)


def params(mib):
    return pltpu.CompilerParams(vmem_limit_bytes=mib * 1024 * 1024)


def from_offset(x, axis, offset):
    count = lax.axis_size(axis)
    return lax.ppermute(x, axis, [((i + offset) % count, i) for i in range(count)])


def after(x, other):
    return lax.optimization_barrier((x, other))[0]


def gathered_parts(own):
    far, up, down = (from_offset(own, X, step) for step in (2, 1, 3))
    mine = (own, up, far, down)
    swapped = []
    for part in (own, up, far, down):
        swapped.append(from_offset(part, CORE, 1))
    return (*mine, *swapped)


def stage_kernel(tokens_ref, gain_ref, staged_tokens_ref, staged_gain_ref):
    staged_tokens_ref[...] = tokens_ref[...]
    staged_gain_ref[...] = gain_ref[...]


def staged(tokens, gain):
    return pl.pallas_call(
        stage_kernel,
        out_shape=(
            jax.ShapeDtypeStruct(tokens.shape, tokens.dtype),
            jax.ShapeDtypeStruct(gain.shape, gain.dtype),
        ),
        in_specs=[VMEM] * 2,
        out_specs=(VMEM,) * 2,
        compiler_params=params(4),
        cost_estimate=pl.CostEstimate(flops=500_000, bytes_accessed=1_000_000, transcendentals=0),
    )(tokens, gain)


def norm_kernel(gain_ref, *refs):
    tokens, normed_ref = refs[:4], refs[4]
    tp = lax.axis_index("tp")
    rows, width = tokens[0].shape
    step_rows = 64

    def norm_step(step, carry):
        at = pl.ds(pl.multiple_of(step * step_rows, step_rows), step_rows)
        blocks = [ref[at, :].astype(jnp.float32) for ref in tokens]
        square = sum(jnp.sum(b * b, axis=1, keepdims=True) for b in blocks)
        scale = lax.rsqrt(square / (4 * width) + norm_eps)
        for k, b in enumerate(blocks):
            cols = pl.ds(pl.multiple_of(lax.rem(tp + k, 4) * width, width), width)
            normed_ref[at, cols] = (b * scale * gain_ref[:, cols]).astype(jnp.bfloat16)
        return carry

    lax.fori_loop(0, rows // step_rows, norm_step, 0)


def normalized(gain, tokens):
    rows, width = tokens[0].shape
    return pl.pallas_call(
        norm_kernel,
        out_shape=jax.ShapeDtypeStruct((rows, 4 * width), jnp.bfloat16),
        in_specs=[VMEM] * 5,
        out_specs=VMEM,
        compiler_params=params(8),
        cost_estimate=pl.CostEstimate(
            flops=500_000_000, bytes_accessed=4_000_000, transcendentals=512
        ),
    )(gain, *tokens)


def place_rows(parts, out_ref, columns):
    x, core = lax.axis_index(X), lax.axis_index(CORE)
    for side in range(2):
        for x_rel in range(4):
            ref = parts[4 * side + x_rel]
            place = lax.rem(x + x_rel, 4) * 2 + lax.rem(core + side, 2)
            for z in range(16):
                at = pl.ds(pl.multiple_of(z * 128 + place * 16, 16), 16)
                out_ref[at, :] = ref[z, :, columns]


def rotated(x, cosine, sine):
    width = x.shape[-1]
    lane = lax.broadcasted_iota(jnp.int32, x.shape, 1)
    ahead = pltpu.roll(x, width - 16, 1)
    behind = pltpu.roll(x, 16, 1)
    return x * cosine + jnp.where(lane % 32 < 16, ahead, behind) * sine


def project_kernel(*refs):
    normed_ref, cos_ref, sin_ref = refs[:3]
    kvc_ref, query_ref, post_ref, out_rows_ref, rows_ref = refs[11:]
    place_rows(refs[3:11], rows_ref, slice(0, 1152))
    place_rows(refs[3:11], out_rows_ref, slice(1152, 1664))

    def projected(first, last):
        return jnp.dot(
            normed_ref[...], rows_ref[:, first:last], preferred_element_type=jnp.float32
        )

    key_value = projected(0, 128)
    lane = lax.broadcasted_iota(jnp.int32, key_value.shape, 1)
    cosine = cos_ref[...]
    sine = sin_ref[...]
    kvc_ref[:, :128] = jnp.where(
        lane < 64, rotated(key_value, cosine, sine), key_value
    ).astype(jnp.bfloat16)
    kvc_ref[:, 128:] = (projected(128, 384) * projected(384, 640)).astype(jnp.bfloat16)
    for half in range(2):
        part = projected(640 + 128 * half, 768 + 128 * half)
        query_ref[:, 128 * half : 128 * (half + 1)] = rotated(part, cosine, sine).astype(
            jnp.bfloat16
        )
    post_ref[...] = projected(896, 1152)


def project(normed, cosine, sine, parts):
    rows = normed.shape[0]
    return pl.pallas_call(
        project_kernel,
        out_shape=(
            jax.ShapeDtypeStruct((rows, 384), jnp.bfloat16),
            jax.ShapeDtypeStruct((rows, 256), jnp.bfloat16),
            jax.ShapeDtypeStruct((rows, 256), jnp.float32),
            jax.ShapeDtypeStruct((2048, 512), jnp.bfloat16),
        ),
        in_specs=[VMEM] * 11,
        out_specs=(VMEM,) * 4,
        scratch_shapes=[pltpu.VMEM((2048, 1152), jnp.bfloat16)],
        compiler_params=params(24),
        cost_estimate=pl.CostEstimate(
            flops=2 * rows * 2048 * 1152, bytes_accessed=8_000_000, transcendentals=0
        ),
    )(normed, cosine, sine, *parts)


def window_bias():
    row = lax.broadcasted_iota(jnp.int32, (WINDOW, 3 * WINDOW), 0)
    col = lax.broadcasted_iota(jnp.int32, (WINDOW, 3 * WINDOW), 1)
    return jnp.where((col >= row) & (col <= row + 2 * WINDOW), 0.0, -jnp.inf)


def inside_sequence(bias, first_key):
    key_pos = first_key + lax.broadcasted_iota(jnp.int32, bias.shape, 1)
    return jnp.where((key_pos >= 0) & (key_pos < TOKENS), bias, -jnp.inf)


def attended_block(query, keys, values, sinks, bias):
    heads = query.shape[1] // HEAD_DIM
    query = query * jnp.bfloat16(HEAD_DIM**-0.5)
    stacked = jnp.concatenate(
        [query[:, HEAD_DIM * h : HEAD_DIM * (h + 1)] for h in range(heads)], axis=0
    )
    scores = lax.dot_general(
        stacked, keys, (((1,), (1,)), ((), ())), preferred_element_type=jnp.float32
    )
    results, logs = [], []
    for h in range(heads):
        own = scores[WINDOW * h : WINDOW * (h + 1)] + bias
        row_max = jnp.maximum(jnp.max(own, axis=1, keepdims=True), sinks[h])
        exp_scores = jnp.exp(own - row_max)
        denominator = jnp.sum(exp_scores, axis=1, keepdims=True) + jnp.exp(sinks[h] - row_max)
        results.append((exp_scores * (1.0 / denominator)).astype(jnp.bfloat16))
        logs.append(row_max + jnp.log(denominator))
    weights = jnp.concatenate(results, axis=0)
    result = jnp.dot(weights, values, preferred_element_type=jnp.float32).astype(jnp.bfloat16)
    return (
        jnp.concatenate([result[WINDOW * h : WINDOW * (h + 1)] for h in range(heads)], axis=1),
        jnp.concatenate(logs, axis=1),
    )


def first_position():
    return lax.axis_index(SP) * 512


def inner_kernel(sink_ref, query_ref, kvc_ref, attended_ref, log_ref):
    sinks = [sink_ref[h] for h in range(4)]
    bias = window_bias()
    for n in (1, 2):
        window = slice((n - 1) * WINDOW, (n + 2) * WINDOW)
        result, log_sum = attended_block(
            query_ref[n * WINDOW : (n + 1) * WINDOW, :],
            kvc_ref[window, :HEAD_DIM],
            kvc_ref[window, HEAD_DIM : 2 * HEAD_DIM],
            sinks,
            bias,
        )
        attended_ref[(n - 1) * WINDOW : n * WINDOW, :] = result
        log_ref[(n - 1) * WINDOW : n * WINDOW, :] = log_sum


def inner(sinks, query, kvc):
    return pl.pallas_call(
        inner_kernel,
        out_shape=(
            jax.ShapeDtypeStruct((256, 256), jnp.bfloat16),
            jax.ShapeDtypeStruct((256, 4), jnp.float32),
        ),
        in_specs=[SMEM, VMEM, VMEM],
        out_specs=(VMEM, VMEM),
        compiler_params=params(12),
        cost_estimate=pl.CostEstimate(
            flops=2 * 2 * 1024 * 384 * 64 * 20, bytes_accessed=2_000_000, transcendentals=400_000
        ),
    )(sinks, query, kvc)


def outer_kernel(
    sink_ref, query_ref, kvc_ref, low_ref, high_ref, post_ref, taps_ref, inner_ref, out_rows_ref,
    *refs,
):
    far_ref, both_ref, log_ref = refs
    sinks = [sink_ref[h] for h in range(4)]
    offset = first_position()
    bias = window_bias()
    rows = query_ref.shape[0]
    edges = (
        (0, jnp.concatenate([low_ref[:, :128], kvc_ref[: 2 * WINDOW, :128]], axis=0)),
        (3, jnp.concatenate([kvc_ref[rows - 2 * WINDOW :, :128], high_ref[:, :128]], axis=0)),
    )
    for k, (n, window) in enumerate(edges):
        result, log_sum = attended_block(
            query_ref[n * WINDOW : (n + 1) * WINDOW, :],
            window[:, :HEAD_DIM],
            window[:, HEAD_DIM:],
            sinks,
            inside_sequence(bias, offset + (n - 1) * WINDOW),
        )
        both_ref[n * WINDOW : (n + 1) * WINDOW, :256] = result
        log_ref[k * WINDOW : (k + 1) * WINDOW, :] = log_sum
    both_ref[WINDOW : 3 * WINDOW, :256] = inner_ref[...]
    conv = kvc_ref[:, 128:].astype(jnp.float32)
    row = lax.broadcasted_iota(jnp.int32, conv.shape, 0)
    before = low_ref[WINDOW - 16 :, 128:].astype(jnp.float32)[15:16]
    after = high_ref[:16, 128:].astype(jnp.float32)[0:1]
    previous = jnp.where(row == 0, before, pltpu.roll(conv, 1, 0))
    following = jnp.where(row == rows - 1, after, pltpu.roll(conv, rows - 1, 0))
    convolved = taps_ref[0:1] * previous + taps_ref[1:2] * conv + taps_ref[2:3] * following
    both_ref[:, 256:] = (post_ref[...] * convolved).astype(jnp.bfloat16)
    far_ref[...] = chunk(both_ref, out_rows_ref, 2).astype(jnp.bfloat16)


def chunk(both_ref, out_rows_ref, step):
    block = lax.rem(lax.axis_index("tp") + step, 4)
    return lax.dot_general(
        both_ref[pl.ds(pl.multiple_of(block * WINDOW, WINDOW), WINDOW), :],
        out_rows_ref[...],
        (((1,), (1,)), ((), ())),
        preferred_element_type=jnp.float32,
    )


def chunk_kernel(step, both_ref, out_rows_ref, out_ref):
    out_ref[...] = chunk(both_ref, out_rows_ref, step).astype(jnp.bfloat16)


def total_kernel(*refs):
    total = refs[0][...].astype(jnp.float32)
    for ref in refs[1:-1]:
        total = total + ref[...].astype(jnp.float32)
    refs[-1][...] = total.astype(jnp.bfloat16)


def rows_out(kernel, *arrays):
    return pl.pallas_call(
        kernel,
        out_shape=jax.ShapeDtypeStruct((128, 2048), jnp.bfloat16),
        in_specs=[VMEM] * len(arrays),
        out_specs=VMEM,
        compiler_params=params(12),
        cost_estimate=pl.CostEstimate(
            flops=2 * 128 * 512 * 2048, bytes_accessed=3_000_000, transcendentals=0
        ),
    )(*arrays)


def outer(sinks, query, kvc, low, high, post, taps, inner_attended, out_rows):
    return pl.pallas_call(
        outer_kernel,
        out_shape=(
            jax.ShapeDtypeStruct((128, 2048), jnp.bfloat16),
            jax.ShapeDtypeStruct((512, 512), jnp.bfloat16),
            jax.ShapeDtypeStruct((256, 4), jnp.float32),
        ),
        in_specs=[SMEM] + [VMEM] * 8,
        out_specs=(VMEM,) * 3,
        compiler_params=params(8),
        cost_estimate=pl.CostEstimate(
            flops=2 * 512 * 512 * 2048, bytes_accessed=8_000_000, transcendentals=400_000
        ),
    )(sinks, query, kvc, low, high, post, taps, inner_attended, out_rows)


def halo(block, width):
    count = lax.axis_size(SP)
    forward = [(i, i + 1) for i in range(count - 1)]
    backward = [(i + 1, i) for i in range(count - 1)]
    low = lax.ppermute(block[-width:], SP, forward)
    high = lax.ppermute(block[:width], SP, backward)
    return low, high


def rotation_tables(rows):
    shape = (rows, 2 * HEAD_DIM)
    lane = lax.broadcasted_iota(jnp.int32, shape, 1)
    position = lax.axis_index(SP) * rows + lax.broadcasted_iota(jnp.int32, shape, 0)
    half_dim = HEAD_DIM // 2
    inv_freq = rope_base ** (-(2 * (lane % 16)).astype(jnp.float32) / half_dim)
    index = jnp.where(lane % HEAD_DIM < half_dim, position // GRID_W, position % GRID_W)
    angle = index.astype(jnp.float32) * inv_freq
    sine = jnp.sin(angle)
    return jnp.cos(angle), jnp.where(lane % half_dim < 16, -sine, sine)


def layer(
    tokens,
    norm_gain,
    w_query,
    w_key,
    w_value,
    w_post_gate,
    w_pre_gate,
    w_conv_in,
    conv_taps,
    sink_logit,
    w_out_attn,
    w_out_conv,
):
    rows = tokens.shape[0]
    piece = jnp.concatenate(
        [
            w_key,
            w_value,
            w_pre_gate,
            w_conv_in,
            w_query,
            w_post_gate,
            w_out_attn.T,
            w_out_conv.T,
        ],
        axis=1,
    )
    cosine, sine = rotation_tables(rows)
    own = lax.all_gather(after(piece, (cosine, sine)), Z, axis=0)
    parts = gathered_parts(own)
    late_tokens = after(tokens, own)
    arrived = [from_offset(late_tokens, "tp", step) for step in (1, 2, 3)]
    own_tokens, gain = staged(tokens, norm_gain[None])
    normed = normalized(gain, [own_tokens, *arrived])
    kvc, query, post, out_rows = project(normed, cosine, sine, parts)
    low, high = halo(kvc, WINDOW)
    inner_attended, inner_log = inner(sink_logit, query, kvc)
    far, both, outer_log = outer(
        sink_logit, query, kvc, low, high, post, conv_taps, inner_attended, out_rows
    )
    arrived = [from_offset(far, "tp", -2)]
    up = rows_out(functools.partial(chunk_kernel, 1), both, out_rows)
    arrived.append(from_offset(up, "tp", -1))
    down = rows_out(functools.partial(chunk_kernel, 3), both, out_rows)
    arrived.append(from_offset(down, "tp", 1))
    mine = rows_out(functools.partial(chunk_kernel, 0), both, out_rows)
    mixed = rows_out(total_kernel, mine, *arrived)
    log_sum = jnp.concatenate([outer_log[:WINDOW], inner_log, outer_log[WINDOW:]])
    return (mixed, log_sum.T)


def solution(mesh):
    torus = Mesh(mesh.devices.reshape(16, 4, 2, mesh.shape["tp"]), SP_TP)
    return jax.shard_map(
        layer,
        mesh=torus,
        in_specs=(
            P(SP, "tp"),
            P(),
            P(SP, "tp"),
            P(SP, "tp"),
            P(SP, "tp"),
            P(SP, "tp"),
            P(SP, "tp"),
            P(SP, "tp"),
            P(None, "tp"),
            P("tp"),
            P("tp", SP),
            P("tp", SP),
        ),
        out_specs=(P(SP_TP, None), P("tp", SP)),
        check_vma=False,
    )
```

profile of v0, /device:TPU:1, one launch (start us, length us, event | category | flops | bytes accessed | tf_op | source)
XLA Modules:
  0.0 153.6 jit_solution(12405134616391701683)
XLA Ops:
  0.7 0.9 concatenate.6
  1.6 1.1 negate_select_fusion
  2.7 34.2 %all-gather = bf16[256,1664]{1,0:T(8,128)(2,1)S(1)} all-gather(bf16[16,1664]{1,0:T(8,128)(2,1)S(1)} %concatenate.6), channel_id=2, replica_groups=mesh['sp_0'=16,'sp_1'=4,'sp_2'=2,'tp'=4] {'sp_0'}, dimensions={0}, use_global_device_ids=true | all-gather | bytes 905216 | tf_op jit(solution)/shard_map/all_gather | solution.py:377
  36.9 3.1 %collective-permute-start.5 = (bf16[16,16,1664]{2,1,0:T(8,128)(2,1)S(1)}, bf16[16,16,1664]{2,1,0:T(8,128)(2,1)S(1)}, u32[]{:S(2)}, u32[]{:S(2)}) collective-permute-start(bf16[16,16,1664]{2,1,0:T(8,128)(2,1)S(1)} %bitcast.6), channel_id=1, source_target_pairs={{24,0},{0,8},{8,16},{16,24},{25,1},{1,9},{9,17},{17,25},{26,2},{2,... | collective-permute-start | bytes 2555912 | tf_op jit(solution)/shard_map/ppermute | solution.py:35
  40.0 4.4 %collective-permute-start.4 = (bf16[16,16,1664]{2,1,0:T(8,128)(2,1)S(1)}, bf16[16,16,1664]{2,1,0:T(8,128)(2,1)S(1)}, u32[]{:S(2)}, u32[]{:S(2)}) collective-permute-start(bf16[16,16,1664]{2,1,0:T(8,128)(2,1)S(1)} %bitcast.7), channel_id=1, source_target_pairs={{16,0},{24,8},{0,16},{8,24},{17,1},{25,9},{1,17},{9,25},{18,2},{26... | collective-permute-start | bytes 2555912 | tf_op jit(solution)/shard_map/ppermute | solution.py:35
  44.4 3.1 %collective-permute-start.3 = (bf16[16,16,1664]{2,1,0:T(8,128)(2,1)S(1)}, bf16[16,16,1664]{2,1,0:T(8,128)(2,1)S(1)}, u32[]{:S(2)}, u32[]{:S(2)}) collective-permute-start(bf16[16,16,1664]{2,1,0:T(8,128)(2,1)S(1)} %bitcast.8), channel_id=1, source_target_pairs={{8,0},{16,8},{24,16},{0,24},{9,1},{17,9},{25,17},{1,25},{10,2},{18... | collective-permute-start | bytes 2555912 | tf_op jit(solution)/shard_map/ppermute | solution.py:35
  47.5 3.2 %collective-permute-start.2 = (bf16[512,512]{1,0:T(8,128)(2,1)}, bf16[512,512]{1,0:T(8,128)(2,1)S(1)}, u32[]{:S(2)}, u32[]{:S(2)}) collective-permute-start(bf16[512,512]{1,0:T(8,128)(2,1)} %tokens_ref.1), channel_id=1, source_target_pairs={{3,0},{0,1},{1,2},{2,3},{7,4},{4,5},{5,6},{6,7},{11,8},{8,9},{9,10... | collective-permute-start | bytes 1572872 | tf_op jit(solution)/shard_map/ppermute | solution.py:35
  50.7 4.5 %collective-permute-start.1 = (bf16[512,512]{1,0:T(8,128)(2,1)}, bf16[512,512]{1,0:T(8,128)(2,1)S(1)}, u32[]{:S(2)}, u32[]{:S(2)}) collective-permute-start(bf16[512,512]{1,0:T(8,128)(2,1)} %tokens_ref.1), channel_id=1, source_target_pairs={{2,0},{3,1},{0,2},{1,3},{6,4},{7,5},{4,6},{5,7},{10,8},{11,9},{8,1... | collective-permute-start | bytes 1572872 | tf_op jit(solution)/shard_map/ppermute | solution.py:35
  55.2 4.0 %collective-permute-done.2.refs_3_ = bf16[512,512]{1,0:T(8,128)(2,1)S(1)} collective-permute-done((bf16[512,512]{1,0:T(8,128)(2,1)}, bf16[512,512]{1,0:T(8,128)(2,1)S(1)}, u32[]{:S(2)}, u32[]{:S(2)}) %collective-permute-start.2) | collective-permute-done | bytes 524320 | tf_op jit(solution)/shard_map/ppermute | solution.py:35
  59.2 14.7 %collective-permute-start.6 = (bf16[16,16,1664]{2,1,0:T(8,128)(2,1)S(1)}, bf16[16,16,1664]{2,1,0:T(8,128)(2,1)S(1)}, u32[]{:S(2)}, u32[]{:S(2)}) collective-permute-start(bf16[16,16,1664]{2,1,0:T(8,128)(2,1)S(1)} %bitcast.9), channel_id=1, source_target_pairs={{4,0},{0,4},{5,1},{1,5},{6,2},{2,6},{7,3},{3,7},{12,8},{8,12},{13,... | collective-permute-start | bytes 2555912 | tf_op jit(solution)/shard_map/ppermute | solution.py:35
  73.9 1.9 %collective-permute-start.9 = (bf16[16,16,1664]{2,1,0:T(8,128)(2,1)S(1)}, bf16[16,16,1664]{2,1,0:T(8,128)(2,1)S(1)}, u32[]{:S(2)}, u32[]{:S(2)}) collective-permute-start(bf16[16,16,1664]{2,1,0:T(8,128)(2,1)S(1)} %collective-permute-done.5.refs_6_), channel_id=1, source_target_pairs={{4,0},{0,4},{5,1},{1,5},{6,2},{2,6},{7,3},{3,7},{12,8},{8,12},{13,... | collective-permute-start | bytes 2555912 | tf_op jit(solution)/shard_map/ppermute | solution.py:35
  75.8 6.7 %collective-permute-start.8 = (bf16[16,16,1664]{2,1,0:T(8,128)(2,1)S(1)}, bf16[16,16,1664]{2,1,0:T(8,128)(2,1)S(1)}, u32[]{:S(2)}, u32[]{:S(2)}) collective-permute-start(bf16[16,16,1664]{2,1,0:T(8,128)(2,1)S(1)} %collective-permute-done.4.refs_5_), channel_id=1, source_target_pairs={{4,0},{0,4},{5,1},{1,5},{6,2},{2,6},{7,3},{3,7},{12,8},{8,12},{13,... | collective-permute-start | bytes 2555912 | tf_op jit(solution)/shard_map/ppermute | solution.py:35
  82.5 1.9 %collective-permute-start.7 = (bf16[16,16,1664]{2,1,0:T(8,128)(2,1)S(1)}, bf16[16,16,1664]{2,1,0:T(8,128)(2,1)S(1)}, u32[]{:S(2)}, u32[]{:S(2)}) collective-permute-start(bf16[16,16,1664]{2,1,0:T(8,128)(2,1)S(1)} %collective-permute-done.3.refs_4_), channel_id=1, source_target_pairs={{4,0},{0,4},{5,1},{1,5},{6,2},{2,6},{7,3},{3,7},{12,8},{8,12},{13,... | collective-permute-start | bytes 2555912 | tf_op jit(solution)/shard_map/ppermute | solution.py:35
  84.5 4.6 %collective-permute-start = (bf16[512,512]{1,0:T(8,128)(2,1)}, bf16[512,512]{1,0:T(8,128)(2,1)S(1)}, u32[]{:S(2)}, u32[]{:S(2)}) collective-permute-start(bf16[512,512]{1,0:T(8,128)(2,1)} %tokens_ref.1), channel_id=1, source_target_pairs={{1,0},{2,1},{3,2},{0,3},{5,4},{6,5},{7,6},{4,7},{9,8},{10,9},{11,1... | collective-permute-start | bytes 1572872 | tf_op jit(solution)/shard_map/ppermute | solution.py:35
  89.1 1.0 copy-done
  90.2 0.7 copy-done.1
  90.9 9.3 %collective-permute-done.refs_1_ = bf16[512,512]{1,0:T(8,128)(2,1)S(1)} collective-permute-done((bf16[512,512]{1,0:T(8,128)(2,1)}, bf16[512,512]{1,0:T(8,128)(2,1)S(1)}, u32[]{:S(2)}, u32[]{:S(2)}) %collective-permute-start) | collective-permute-done | bytes 524320 | tf_op jit(solution)/shard_map/ppermute | solution.py:35
  100.2 1.4 shard_map.132.refs_0_
  101.7 4.0 %shard_map.133 = (bf16[512,384]{1,0:T(8,128)(2,1)S(1)}, bf16[512,256]{1,0:T(8,128)(2,1)S(1)}, f32[512,256]{1,0:T(8,128)S(1)}, bf16[2048,512]{1,0:T(8,128)(2,1)S(1)}) custom-call(bf16[512,2048]{1,0:T(8,128)(2,1)S(1)} %shard_map.132.refs_0_, f32[512,128]{1,0:T(8,128)S(1)} %get-tuple-element.35.refs_1_, f32[512,128]{1,0:T(8,128)S(1)} %get-tuple-element.34.refs_2_, ...), custom_call_target="tpu_custom_call" | custom-call | flops 2415919104 | bytes 8000000 | tf_op jit(solution)/shard_map/pallas_call | solution.py:151
  105.7 3.3 %collective-permute-start.11 = (bf16[128,384]{1,0:T(8,128)(2,1)S(1)}, bf16[128,384]{1,0:T(8,128)(2,1)S(1)}, u32[]{:S(2)}, u32[]{:S(2)}) collective-permute-start(bf16[128,384]{1,0:T(8,128)(2,1)S(1)} %get-tuple-element.30), channel_id=1, source_target_pairs={{4,0},{8,4},{12,8},{16,12},{20,16},{24,20},{28,24},{32,28},{36,32}... | collective-permute-start | bytes 294920 | tf_op jit(solution)/shard_map/ppermute | solution.py:332
  109.0 3.5 %collective-permute-start.10 = (bf16[128,384]{1,0:T(8,128)(2,1)S(1)}, bf16[128,384]{1,0:T(8,128)(2,1)S(1)}, u32[]{:S(2)}, u32[]{:S(2)}) collective-permute-start(bf16[128,384]{1,0:T(8,128)(2,1)S(1)} %get-tuple-element.31), channel_id=1, source_target_pairs={{0,4},{4,8},{8,12},{12,16},{16,20},{20,24},{24,28},{28,32},{32,36}... | collective-permute-start | bytes 294920 | tf_op jit(solution)/shard_map/ppermute | solution.py:331
  112.5 2.1 %shard_map.134 = (bf16[256,256]{1,0:T(8,128)(2,1)S(1)}, f32[256,4]{1,0:T(8,128)S(1)}) custom-call(f32[4]{0:T(128)S(1)} %copy-done.3, bf16[512,256]{1,0:T(8,128)(2,1)S(1)} %get-tuple-element.19.query_ref, bf16[512,384]{1,0:T(8,128)(2,1)S(1)} %get-tuple-element.20.kvc_ref), custom_call_target="tpu_custom_call" | custom-call | flops 2013265920 | bytes 2000000 | tf_op jit(solution)/shard_map/pallas_call | solution.py:226
  114.6 3.7 %shard_map.135 = (bf16[128,2048]{1,0:T(8,128)(2,1)}, bf16[512,512]{1,0:T(8,128)(2,1)S(1)}, f32[256,4]{1,0:T(8,128)S(1)}) custom-call(f32[4]{0:T(128)S(1)} %copy-done.3, bf16[512,256]{1,0:T(8,128)(2,1)S(1)} %get-tuple-element.19.query_ref, bf16[512,384]{1,0:T(8,128)(2,1)S(1)} %get-tuple-element.20.kvc_ref, ...), custom_call_target="tpu_custom_call" | custom-call | flops 1073741824 | bytes 8000000 | tf_op jit(solution)/shard_map/pallas_call | solution.py:311
  118.3 1.6 %shard_map.138 = bf16[128,2048]{1,0:T(8,128)(2,1)} custom-call(bf16[512,512]{1,0:T(8,128)(2,1)S(1)} %get-tuple-element.24.both_ref, bf16[2048,512]{1,0:T(8,128)(2,1)S(1)} %get-tuple-element.23.out_rows_ref), custom_call_target="tpu_custom_call" | custom-call | flops 268435456 | bytes 3000000 | tf_op jit(solution)/shard_map/pallas_call | solution.py:298
  119.9 1.6 %shard_map.137 = bf16[128,2048]{1,0:T(8,128)(2,1)} custom-call(bf16[512,512]{1,0:T(8,128)(2,1)S(1)} %get-tuple-element.24.both_ref, bf16[2048,512]{1,0:T(8,128)(2,1)S(1)} %get-tuple-element.23.out_rows_ref), custom_call_target="tpu_custom_call" | custom-call | flops 268435456 | bytes 3000000 | tf_op jit(solution)/shard_map/pallas_call | solution.py:298
  121.5 2.6 %collective-permute-start.13 = (bf16[128,2048]{1,0:T(8,128)(2,1)}, bf16[128,2048]{1,0:T(8,128)(2,1)S(1)}, u32[]{:S(2)}, u32[]{:S(2)}) collective-permute-start(bf16[128,2048]{1,0:T(8,128)(2,1)} %shard_map.137), channel_id=1, source_target_pairs={{3,0},{0,1},{1,2},{2,3},{7,4},{4,5},{5,6},{6,7},{11,8},{8,9},{9,10... | collective-permute-start | bytes 1572872 | tf_op jit(solution)/shard_map/ppermute | solution.py:35
  124.1 4.5 %collective-permute-start.14 = (bf16[128,2048]{1,0:T(8,128)(2,1)}, bf16[128,2048]{1,0:T(8,128)(2,1)}, u32[]{:S(2)}, u32[]{:S(2)}) collective-permute-start(bf16[128,2048]{1,0:T(8,128)(2,1)} %shard_map.138), channel_id=1, source_target_pairs={{1,0},{2,1},{3,2},{0,3},{5,4},{6,5},{7,6},{4,7},{9,8},{10,9},{11,1... | collective-permute-start | bytes 1572872 | tf_op jit(solution)/shard_map/ppermute | solution.py:35
  128.7 3.1 %collective-permute-start.12 = (bf16[128,2048]{1,0:T(8,128)(2,1)}, bf16[128,2048]{1,0:T(8,128)(2,1)}, u32[]{:S(2)}, u32[]{:S(2)}) collective-permute-start(bf16[128,2048]{1,0:T(8,128)(2,1)} %get-tuple-element.25), channel_id=1, source_target_pairs={{2,0},{3,1},{0,2},{1,3},{6,4},{7,5},{4,6},{5,7},{10,8},{11,9},{8,1... | collective-permute-start | bytes 1572872 | tf_op jit(solution)/shard_map/ppermute | solution.py:35
  132.0 0.8 shard_map.136.refs_0_
  133.5 4.8 %collective-permute-done.13.refs_2_ = bf16[128,2048]{1,0:T(8,128)(2,1)S(1)} collective-permute-done((bf16[128,2048]{1,0:T(8,128)(2,1)}, bf16[128,2048]{1,0:T(8,128)(2,1)S(1)}, u32[]{:S(2)}, u32[]{:S(2)}) %collective-permute-start.13) | collective-permute-done | bytes 524320 | tf_op jit(solution)/shard_map/ppermute | solution.py:35
  138.2 13.1 %collective-permute-done.14.refs_3_ = bf16[128,2048]{1,0:T(8,128)(2,1)} collective-permute-done((bf16[128,2048]{1,0:T(8,128)(2,1)}, bf16[128,2048]{1,0:T(8,128)(2,1)}, u32[]{:S(2)}, u32[]{:S(2)}) %collective-permute-start.14) | collective-permute-done | bytes 524320 | tf_op jit(solution)/shard_map/ppermute | solution.py:35
  151.3 2.2 %shard_map.139 = bf16[128,2048]{1,0:T(8,128)(2,1)} custom-call(bf16[128,2048]{1,0:T(8,128)(2,1)S(1)} %shard_map.136.refs_0_, bf16[128,2048]{1,0:T(8,128)(2,1)} %collective-permute-done.12.refs_1_, bf16[128,2048]{1,0:T(8,128)(2,1)S(1)} %collective-permute-done.13.refs_2_, bf16[128,2048]{1,0:T(8,128)(2,1)} %collective-permute-done.14.refs_3_), custom_call_target="tpu_custom_call" | custom-call | flops 268435456 | bytes 3000000 | tf_op jit(solution)/shard_map/pallas_call | solution.py:298
  (32 shorter events, 1.0 us)
Async XLA Ops:
  36.9 37.0 %collective-permute-start.5 = (bf16[16,16,1664]{2,1,0:T(8,128)(2,1)S(1)}, bf16[16,16,1664]{2,1,0:T(8,128)(2,1)S(1)}, u32[]{:S(2)}, u32[]{:S(2)}) collective-permute-start(bf16[16,16,1664]{2,1,0:T(8,128)(2,1)S(1)} %bitcast.6), channel_id=1, source_target_pairs={{24,0},{0,8},{8,16},{16,24},{25,1},{1,9},{9,17},{17,25},{26,2},{2,... | collective-permute-start | bytes 2555912 | tf_op jit(solution)/shard_map/ppermute | solution.py:35
  40.0 35.8 %collective-permute-start.4 = (bf16[16,16,1664]{2,1,0:T(8,128)(2,1)S(1)}, bf16[16,16,1664]{2,1,0:T(8,128)(2,1)S(1)}, u32[]{:S(2)}, u32[]{:S(2)}) collective-permute-start(bf16[16,16,1664]{2,1,0:T(8,128)(2,1)S(1)} %bitcast.7), channel_id=1, source_target_pairs={{16,0},{24,8},{0,16},{8,24},{17,1},{25,9},{1,17},{9,25},{18,2},{26... | collective-permute-start | bytes 2555912 | tf_op jit(solution)/shard_map/ppermute | solution.py:35
  44.4 38.1 %collective-permute-start.3 = (bf16[16,16,1664]{2,1,0:T(8,128)(2,1)S(1)}, bf16[16,16,1664]{2,1,0:T(8,128)(2,1)S(1)}, u32[]{:S(2)}, u32[]{:S(2)}) collective-permute-start(bf16[16,16,1664]{2,1,0:T(8,128)(2,1)S(1)} %bitcast.8), channel_id=1, source_target_pairs={{8,0},{16,8},{24,16},{0,24},{9,1},{17,9},{25,17},{1,25},{10,2},{18... | collective-permute-start | bytes 2555912 | tf_op jit(solution)/shard_map/ppermute | solution.py:35
  47.5 11.7 %collective-permute-start.2 = (bf16[512,512]{1,0:T(8,128)(2,1)}, bf16[512,512]{1,0:T(8,128)(2,1)S(1)}, u32[]{:S(2)}, u32[]{:S(2)}) collective-permute-start(bf16[512,512]{1,0:T(8,128)(2,1)} %tokens_ref.1), channel_id=1, source_target_pairs={{3,0},{0,1},{1,2},{2,3},{7,4},{4,5},{5,6},{6,7},{11,8},{8,9},{9,10... | collective-permute-start | bytes 1572872 | tf_op jit(solution)/shard_map/ppermute | solution.py:35
  50.7 33.8 %collective-permute-start.1 = (bf16[512,512]{1,0:T(8,128)(2,1)}, bf16[512,512]{1,0:T(8,128)(2,1)S(1)}, u32[]{:S(2)}, u32[]{:S(2)}) collective-permute-start(bf16[512,512]{1,0:T(8,128)(2,1)} %tokens_ref.1), channel_id=1, source_target_pairs={{2,0},{3,1},{0,2},{1,3},{6,4},{7,5},{4,6},{5,7},{10,8},{11,9},{8,1... | collective-permute-start | bytes 1572872 | tf_op jit(solution)/shard_map/ppermute | solution.py:35
  59.2 42.5 %collective-permute-start.6 = (bf16[16,16,1664]{2,1,0:T(8,128)(2,1)S(1)}, bf16[16,16,1664]{2,1,0:T(8,128)(2,1)S(1)}, u32[]{:S(2)}, u32[]{:S(2)}) collective-permute-start(bf16[16,16,1664]{2,1,0:T(8,128)(2,1)S(1)} %bitcast.9), channel_id=1, source_target_pairs={{4,0},{0,4},{5,1},{1,5},{6,2},{2,6},{7,3},{3,7},{12,8},{8,12},{13,... | collective-permute-start | bytes 2555912 | tf_op jit(solution)/shard_map/ppermute | solution.py:35
  73.9 27.8 %collective-permute-start.9 = (bf16[16,16,1664]{2,1,0:T(8,128)(2,1)S(1)}, bf16[16,16,1664]{2,1,0:T(8,128)(2,1)S(1)}, u32[]{:S(2)}, u32[]{:S(2)}) collective-permute-start(bf16[16,16,1664]{2,1,0:T(8,128)(2,1)S(1)} %collective-permute-done.5.refs_6_), channel_id=1, source_target_pairs={{4,0},{0,4},{5,1},{1,5},{6,2},{2,6},{7,3},{3,7},{12,8},{8,12},{13,... | collective-permute-start | bytes 2555912 | tf_op jit(solution)/shard_map/ppermute | solution.py:35
  75.8 25.8 %collective-permute-start.8 = (bf16[16,16,1664]{2,1,0:T(8,128)(2,1)S(1)}, bf16[16,16,1664]{2,1,0:T(8,128)(2,1)S(1)}, u32[]{:S(2)}, u32[]{:S(2)}) collective-permute-start(bf16[16,16,1664]{2,1,0:T(8,128)(2,1)S(1)} %collective-permute-done.4.refs_5_), channel_id=1, source_target_pairs={{4,0},{0,4},{5,1},{1,5},{6,2},{2,6},{7,3},{3,7},{12,8},{8,12},{13,... | collective-permute-start | bytes 2555912 | tf_op jit(solution)/shard_map/ppermute | solution.py:35
  82.5 19.1 %collective-permute-start.7 = (bf16[16,16,1664]{2,1,0:T(8,128)(2,1)S(1)}, bf16[16,16,1664]{2,1,0:T(8,128)(2,1)S(1)}, u32[]{:S(2)}, u32[]{:S(2)}) collective-permute-start(bf16[16,16,1664]{2,1,0:T(8,128)(2,1)S(1)} %collective-permute-done.3.refs_4_), channel_id=1, source_target_pairs={{4,0},{0,4},{5,1},{1,5},{6,2},{2,6},{7,3},{3,7},{12,8},{8,12},{13,... | collective-permute-start | bytes 2555912 | tf_op jit(solution)/shard_map/ppermute | solution.py:35
  84.5 15.7 %collective-permute-start = (bf16[512,512]{1,0:T(8,128)(2,1)}, bf16[512,512]{1,0:T(8,128)(2,1)S(1)}, u32[]{:S(2)}, u32[]{:S(2)}) collective-permute-start(bf16[512,512]{1,0:T(8,128)(2,1)} %tokens_ref.1), channel_id=1, source_target_pairs={{1,0},{2,1},{3,2},{0,3},{5,4},{6,5},{7,6},{4,7},{9,8},{10,9},{11,1... | collective-permute-start | bytes 1572872 | tf_op jit(solution)/shard_map/ppermute | solution.py:35
  89.1 1.1 copy-start
  90.2 0.7 copy-start.1
  101.6 10.9 %copy-start.3 = (f32[4]{0:T(128)S(1)}, f32[4]{0:T(128)}, u32[]{:S(2)}) copy-start(f32[4]{0:T(128)} %sink_ref.3) | copy-start | bytes 52
  105.7 8.9 %collective-permute-start.11 = (bf16[128,384]{1,0:T(8,128)(2,1)S(1)}, bf16[128,384]{1,0:T(8,128)(2,1)S(1)}, u32[]{:S(2)}, u32[]{:S(2)}) collective-permute-start(bf16[128,384]{1,0:T(8,128)(2,1)S(1)} %get-tuple-element.30), channel_id=1, source_target_pairs={{4,0},{8,4},{12,8},{16,12},{20,16},{24,20},{28,24},{32,28},{36,32}... | collective-permute-start | bytes 294920 | tf_op jit(solution)/shard_map/ppermute | solution.py:332
  109.0 5.6 %collective-permute-start.10 = (bf16[128,384]{1,0:T(8,128)(2,1)S(1)}, bf16[128,384]{1,0:T(8,128)(2,1)S(1)}, u32[]{:S(2)}, u32[]{:S(2)}) collective-permute-start(bf16[128,384]{1,0:T(8,128)(2,1)S(1)} %get-tuple-element.31), channel_id=1, source_target_pairs={{0,4},{4,8},{8,12},{12,16},{16,20},{20,24},{24,28},{28,32},{32,36}... | collective-permute-start | bytes 294920 | tf_op jit(solution)/shard_map/ppermute | solution.py:331
  112.5 2.1 %copy-start.2 = (f32[3,256]{1,0:T(4,128)S(1)}, f32[3,256]{1,0:T(4,128)}, u32[]{:S(2)}) copy-start(f32[3,256]{1,0:T(4,128)} %taps_ref.1) | copy-start | bytes 9220
  121.5 16.7 %collective-permute-start.13 = (bf16[128,2048]{1,0:T(8,128)(2,1)}, bf16[128,2048]{1,0:T(8,128)(2,1)S(1)}, u32[]{:S(2)}, u32[]{:S(2)}) collective-permute-start(bf16[128,2048]{1,0:T(8,128)(2,1)} %shard_map.137), channel_id=1, source_target_pairs={{3,0},{0,1},{1,2},{2,3},{7,4},{4,5},{5,6},{6,7},{11,8},{8,9},{9,10... | collective-permute-start | bytes 1572872 | tf_op jit(solution)/shard_map/ppermute | solution.py:35
  124.1 27.2 %collective-permute-start.14 = (bf16[128,2048]{1,0:T(8,128)(2,1)}, bf16[128,2048]{1,0:T(8,128)(2,1)}, u32[]{:S(2)}, u32[]{:S(2)}) collective-permute-start(bf16[128,2048]{1,0:T(8,128)(2,1)} %shard_map.138), channel_id=1, source_target_pairs={{1,0},{2,1},{3,2},{0,3},{5,4},{6,5},{7,6},{4,7},{9,8},{10,9},{11,1... | collective-permute-start | bytes 1572872 | tf_op jit(solution)/shard_map/ppermute | solution.py:35
  128.7 22.7 %collective-permute-start.12 = (bf16[128,2048]{1,0:T(8,128)(2,1)}, bf16[128,2048]{1,0:T(8,128)(2,1)}, u32[]{:S(2)}, u32[]{:S(2)}) collective-permute-start(bf16[128,2048]{1,0:T(8,128)(2,1)} %get-tuple-element.25), channel_id=1, source_target_pairs={{2,0},{3,1},{0,2},{1,3},{6,4},{7,5},{4,6},{5,7},{10,8},{11,9},{8,1... | collective-permute-start | bytes 1572872 | tf_op jit(solution)/shard_map/ppermute | solution.py:35
where the time goes:
time: 156 us; the launch traced here: 154 us
  starting transfers between devices  65.1 us (42%)
  blocking collectives  34.2 us (22%)
  waiting for transfers between devices  31.2 us (20%)
  Pallas kernels  17.5 us (11%)
  local copies, waits for them, and re-layouts  2.91 us (2%)
  other arithmetic  1.72 us (1%)
    ppermute x13, starting transfers between devices, from_offset(): lax.ppermute(x, axis, [((i + offset) % count, i) for i in range(count)])  58.3 us
    all_gather x1, blocking collectives, layer(): own = lax.all_gather(after(piece, (cosine, sine)), Z, axis=0)  34.2 us
    ppermute x13, waiting for transfers between devices, from_offset(): lax.ppermute(x, axis, [((i + offset) % count, i) for i in range(count)])  31.2 us
    pallas_call x4, Pallas kernels, rows_out(): pl.pallas_call(kernel, out_shape=jax.ShapeDtypeStruct((128, 2048), jnp.bf...  6.32 us
    pallas_call x1, Pallas kernels, project(): pl.pallas_call(project_kernel, out_shape=(jax.ShapeDtypeStruct((rows, 384...  3.98 us
    pallas_call x1, Pallas kernels, outer(): pl.pallas_call(outer_kernel, out_shape=(jax.ShapeDtypeStruct((128, 2048),...  3.69 us
    ppermute x1, starting transfers between devices, halo(): low = lax.ppermute(block[-width:], SP, forward)  3.51 us
    ppermute x1, starting transfers between devices, halo(): high = lax.ppermute(block[:width], SP, backward)  3.26 us
  transfers between devices with their start and end apart: 15, of which 4 were waited for; matrix products, arithmetic and copies ran while one was open for 1% of the time, Pallas kernels for 3%

commit v1 on v0

--- a/solution.py
+++ b/solution.py
@@ -1,5 +1,3 @@
-import functools
-
 import jax
 import jax.numpy as jnp
 from jax import lax
@@ -40,7 +38,8 @@
 
 
 def gathered_parts(own):
-    far, up, down = (from_offset(own, X, step) for step in (2, 1, 3))
+    far = from_offset(own, X, 2)
+    up, down = from_offset(own, X, 1), from_offset(own, X, 3)
     mine = (own, up, far, down)
     swapped = []
     for part in (own, up, far, down):
@@ -283,26 +282,24 @@
     )
 
 
-def chunk_kernel(step, both_ref, out_rows_ref, out_ref):
-    out_ref[...] = chunk(both_ref, out_rows_ref, step).astype(jnp.bfloat16)
-
-
-def total_kernel(*refs):
-    total = refs[0][...].astype(jnp.float32)
-    for ref in refs[1:-1]:
-        total = total + ref[...].astype(jnp.float32)
-    refs[-1][...] = total.astype(jnp.bfloat16)
-
-
-def rows_out(kernel, *arrays):
+def near_kernel(both_ref, out_rows_ref, up_ref, down_ref):
+    up_ref[...] = chunk(both_ref, out_rows_ref, 1).astype(jnp.bfloat16)
+    down_ref[...] = chunk(both_ref, out_rows_ref, 3).astype(jnp.bfloat16)
+
+
+def own_kernel(both_ref, out_rows_ref, own_ref):
+    own_ref[...] = chunk(both_ref, out_rows_ref, 0).astype(jnp.bfloat16)
+
+
+def chunks(kernel, count, *arrays):
     return pl.pallas_call(
         kernel,
-        out_shape=jax.ShapeDtypeStruct((128, 2048), jnp.bfloat16),
+        out_shape=(jax.ShapeDtypeStruct((128, 2048), jnp.bfloat16),) * count,
         in_specs=[VMEM] * len(arrays),
-        out_specs=VMEM,
+        out_specs=(VMEM,) * count,
         compiler_params=params(12),
         cost_estimate=pl.CostEstimate(
-            flops=2 * 128 * 512 * 2048, bytes_accessed=3_000_000, transcendentals=0
+            flops=count * 2 * 128 * 512 * 2048, bytes_accessed=3_000_000, transcendentals=0
         ),
     )(*arrays)
 
@@ -387,14 +384,14 @@
         sink_logit, query, kvc, low, high, post, conv_taps, inner_attended, out_rows
     )
     arrived = [from_offset(far, "tp", -2)]
-    up = rows_out(functools.partial(chunk_kernel, 1), both, out_rows)
-    arrived.append(from_offset(up, "tp", -1))
-    down = rows_out(functools.partial(chunk_kernel, 3), both, out_rows)
-    arrived.append(from_offset(down, "tp", 1))
-    mine = rows_out(functools.partial(chunk_kernel, 0), both, out_rows)
-    mixed = rows_out(total_kernel, mine, *arrived)
+    up, down = chunks(near_kernel, 2, both, out_rows)
+    arrived += [from_offset(up, "tp", -1), from_offset(down, "tp", 1)]
+    (mine,) = chunks(own_kernel, 1, both, out_rows)
+    total = mine.astype(jnp.float32)
+    for block in arrived:
+        total = total + block.astype(jnp.float32)
     log_sum = jnp.concatenate([outer_log[:WINDOW], inner_log, outer_log[WINDOW:]])
-    return (mixed, log_sum.T)
+    return (total.astype(jnp.bfloat16), log_sum.T)
 
 
 def solution(mesh):

time: 156 us -> 155 us (level)
  Pallas kernels: 17.5 us -> 13.5 us
  other arithmetic: 1.72 us -> 4.21 us
    pallas_call x4 -> x2, Pallas kernels: 6.32 us -> 3.09 us  [chunks(): pl.pallas_call(kernel, out_shape=(jax.ShapeDtypeStruct((128, 2048), jnp.b...]
    convert_element_type x0 -> x1, other arithmetic: none -> 2.48 us  [layer(): return (total.astype(jnp.bfloat16), log_sum.T)]
where the time goes in v1:
time: 155 us; the launch traced here: 152 us
  starting transfers between devices  65.1 us (42%)
  blocking collectives  34.2 us (22%)
  waiting for transfers between devices  31.2 us (20%)
  Pallas kernels  13.5 us (9%)
  other arithmetic  4.21 us (3%)
  local copies, waits for them, and re-layouts  2.91 us (2%)
    ppermute x13, starting transfers between devices, from_offset(): lax.ppermute(x, axis, [((i + offset) % count, i) for i in range(count)])  58.3 us
    all_gather x1, blocking collectives, layer(): own = lax.all_gather(after(piece, (cosine, sine)), Z, axis=0)  34.2 us
    ppermute x13, waiting for transfers between devices, from_offset(): lax.ppermute(x, axis, [((i + offset) % count, i) for i in range(count)])  31.2 us
    pallas_call x1, Pallas kernels, project(): pl.pallas_call(project_kernel, out_shape=(jax.ShapeDtypeStruct((rows, 384...  3.98 us
    ppermute x1, starting transfers between devices, halo(): low = lax.ppermute(block[-width:], SP, forward)  3.51 us
    ppermute x1, starting transfers between devices, halo(): high = lax.ppermute(block[:width], SP, backward)  3.26 us
  transfers between devices with their start and end apart: 15, of which 4 were waited for; matrix products, arithmetic and copies ran while one was open for 1% of the time, Pallas kernels for 3%

profile of v1, /device:TPU:1, one launch (start us, length us, event | category | flops | bytes accessed | tf_op | source)
XLA Modules:
  0.0 152.1 jit_solution(15360571855798431569)
XLA Ops:
  0.7 0.9 concatenate.6
  1.6 1.1 negate_select_fusion
  2.7 34.2 %all-gather = bf16[256,1664]{1,0:T(8,128)(2,1)S(1)} all-gather(bf16[16,1664]{1,0:T(8,128)(2,1)S(1)} %concatenate.6), channel_id=2, replica_groups=mesh['sp_0'=16,'sp_1'=4,'sp_2'=2,'tp'=4] {'sp_0'}, dimensions={0}, use_global_device_ids=true | all-gather | bytes 905216 | tf_op jit(solution)/shard_map/all_gather | solution.py:374
  36.9 3.1 %collective-permute-start.5 = (bf16[16,16,1664]{2,1,0:T(8,128)(2,1)S(1)}, bf16[16,16,1664]{2,1,0:T(8,128)(2,1)S(1)}, u32[]{:S(2)}, u32[]{:S(2)}) collective-permute-start(bf16[16,16,1664]{2,1,0:T(8,128)(2,1)S(1)} %bitcast.6), channel_id=1, source_target_pairs={{24,0},{0,8},{8,16},{16,24},{25,1},{1,9},{9,17},{17,25},{26,2},{2,... | collective-permute-start | bytes 2555912 | tf_op jit(solution)/shard_map/ppermute | solution.py:33
  40.0 4.4 %collective-permute-start.4 = (bf16[16,16,1664]{2,1,0:T(8,128)(2,1)S(1)}, bf16[16,16,1664]{2,1,0:T(8,128)(2,1)S(1)}, u32[]{:S(2)}, u32[]{:S(2)}) collective-permute-start(bf16[16,16,1664]{2,1,0:T(8,128)(2,1)S(1)} %bitcast.7), channel_id=1, source_target_pairs={{16,0},{24,8},{0,16},{8,24},{17,1},{25,9},{1,17},{9,25},{18,2},{26... | collective-permute-start | bytes 2555912 | tf_op jit(solution)/shard_map/ppermute | solution.py:33
  44.4 3.1 %collective-permute-start.3 = (bf16[16,16,1664]{2,1,0:T(8,128)(2,1)S(1)}, bf16[16,16,1664]{2,1,0:T(8,128)(2,1)S(1)}, u32[]{:S(2)}, u32[]{:S(2)}) collective-permute-start(bf16[16,16,1664]{2,1,0:T(8,128)(2,1)S(1)} %bitcast.8), channel_id=1, source_target_pairs={{8,0},{16,8},{24,16},{0,24},{9,1},{17,9},{25,17},{1,25},{10,2},{18... | collective-permute-start | bytes 2555912 | tf_op jit(solution)/shard_map/ppermute | solution.py:33
  47.5 3.2 %collective-permute-start.2 = (bf16[512,512]{1,0:T(8,128)(2,1)}, bf16[512,512]{1,0:T(8,128)(2,1)S(1)}, u32[]{:S(2)}, u32[]{:S(2)}) collective-permute-start(bf16[512,512]{1,0:T(8,128)(2,1)} %tokens_ref.1), channel_id=1, source_target_pairs={{3,0},{0,1},{1,2},{2,3},{7,4},{4,5},{5,6},{6,7},{11,8},{8,9},{9,10... | collective-permute-start | bytes 1572872 | tf_op jit(solution)/shard_map/ppermute | solution.py:33
  50.7 4.5 %collective-permute-start.1 = (bf16[512,512]{1,0:T(8,128)(2,1)}, bf16[512,512]{1,0:T(8,128)(2,1)S(1)}, u32[]{:S(2)}, u32[]{:S(2)}) collective-permute-start(bf16[512,512]{1,0:T(8,128)(2,1)} %tokens_ref.1), channel_id=1, source_target_pairs={{2,0},{3,1},{0,2},{1,3},{6,4},{7,5},{4,6},{5,7},{10,8},{11,9},{8,1... | collective-permute-start | bytes 1572872 | tf_op jit(solution)/shard_map/ppermute | solution.py:33
  55.2 4.0 %collective-permute-done.2.refs_3_ = bf16[512,512]{1,0:T(8,128)(2,1)S(1)} collective-permute-done((bf16[512,512]{1,0:T(8,128)(2,1)}, bf16[512,512]{1,0:T(8,128)(2,1)S(1)}, u32[]{:S(2)}, u32[]{:S(2)}) %collective-permute-start.2) | collective-permute-done | bytes 524320 | tf_op jit(solution)/shard_map/ppermute | solution.py:33
  59.2 14.7 %collective-permute-start.6 = (bf16[16,16,1664]{2,1,0:T(8,128)(2,1)S(1)}, bf16[16,16,1664]{2,1,0:T(8,128)(2,1)S(1)}, u32[]{:S(2)}, u32[]{:S(2)}) collective-permute-start(bf16[16,16,1664]{2,1,0:T(8,128)(2,1)S(1)} %bitcast.9), channel_id=1, source_target_pairs={{4,0},{0,4},{5,1},{1,5},{6,2},{2,6},{7,3},{3,7},{12,8},{8,12},{13,... | collective-permute-start | bytes 2555912 | tf_op jit(solution)/shard_map/ppermute | solution.py:33
  73.9 1.9 %collective-permute-start.9 = (bf16[16,16,1664]{2,1,0:T(8,128)(2,1)S(1)}, bf16[16,16,1664]{2,1,0:T(8,128)(2,1)S(1)}, u32[]{:S(2)}, u32[]{:S(2)}) collective-permute-start(bf16[16,16,1664]{2,1,0:T(8,128)(2,1)S(1)} %collective-permute-done.5.refs_6_), channel_id=1, source_target_pairs={{4,0},{0,4},{5,1},{1,5},{6,2},{2,6},{7,3},{3,7},{12,8},{8,12},{13,... | collective-permute-start | bytes 2555912 | tf_op jit(solution)/shard_map/ppermute | solution.py:33
  75.8 6.7 %collective-permute-start.8 = (bf16[16,16,1664]{2,1,0:T(8,128)(2,1)S(1)}, bf16[16,16,1664]{2,1,0:T(8,128)(2,1)S(1)}, u32[]{:S(2)}, u32[]{:S(2)}) collective-permute-start(bf16[16,16,1664]{2,1,0:T(8,128)(2,1)S(1)} %collective-permute-done.4.refs_5_), channel_id=1, source_target_pairs={{4,0},{0,4},{5,1},{1,5},{6,2},{2,6},{7,3},{3,7},{12,8},{8,12},{13,... | collective-permute-start | bytes 2555912 | tf_op jit(solution)/shard_map/ppermute | solution.py:33
  82.5 1.9 %collective-permute-start.7 = (bf16[16,16,1664]{2,1,0:T(8,128)(2,1)S(1)}, bf16[16,16,1664]{2,1,0:T(8,128)(2,1)S(1)}, u32[]{:S(2)}, u32[]{:S(2)}) collective-permute-start(bf16[16,16,1664]{2,1,0:T(8,128)(2,1)S(1)} %collective-permute-done.3.refs_4_), channel_id=1, source_target_pairs={{4,0},{0,4},{5,1},{1,5},{6,2},{2,6},{7,3},{3,7},{12,8},{8,12},{13,... | collective-permute-start | bytes 2555912 | tf_op jit(solution)/shard_map/ppermute | solution.py:33
  84.5 4.6 %collective-permute-start = (bf16[512,512]{1,0:T(8,128)(2,1)}, bf16[512,512]{1,0:T(8,128)(2,1)S(1)}, u32[]{:S(2)}, u32[]{:S(2)}) collective-permute-start(bf16[512,512]{1,0:T(8,128)(2,1)} %tokens_ref.1), channel_id=1, source_target_pairs={{1,0},{2,1},{3,2},{0,3},{5,4},{6,5},{7,6},{4,7},{9,8},{10,9},{11,1... | collective-permute-start | bytes 1572872 | tf_op jit(solution)/shard_map/ppermute | solution.py:33
  89.1 1.0 copy-done
  90.2 0.7 copy-done.1
  90.9 9.3 %collective-permute-done.refs_1_ = bf16[512,512]{1,0:T(8,128)(2,1)S(1)} collective-permute-done((bf16[512,512]{1,0:T(8,128)(2,1)}, bf16[512,512]{1,0:T(8,128)(2,1)S(1)}, u32[]{:S(2)}, u32[]{:S(2)}) %collective-permute-start) | collective-permute-done | bytes 524320 | tf_op jit(solution)/shard_map/ppermute | solution.py:33
  100.2 1.4 shard_map.132.refs_0_
  101.7 4.0 %shard_map.133 = (bf16[512,384]{1,0:T(8,128)(2,1)S(1)}, bf16[512,256]{1,0:T(8,128)(2,1)S(1)}, f32[512,256]{1,0:T(8,128)S(1)}, bf16[2048,512]{1,0:T(8,128)(2,1)S(1)}) custom-call(bf16[512,2048]{1,0:T(8,128)(2,1)S(1)} %shard_map.132.refs_0_, f32[512,128]{1,0:T(8,128)S(1)} %get-tuple-element.39.refs_1_, f32[512,128]{1,0:T(8,128)S(1)} %get-tuple-element.38.refs_2_, ...), custom_call_target="tpu_custom_call" | custom-call | flops 2415919104 | bytes 8000000 | tf_op jit(solution)/shard_map/pallas_call | solution.py:150
  105.7 3.3 %collective-permute-start.11 = (bf16[128,384]{1,0:T(8,128)(2,1)S(1)}, bf16[128,384]{1,0:T(8,128)(2,1)S(1)}, u32[]{:S(2)}, u32[]{:S(2)}) collective-permute-start(bf16[128,384]{1,0:T(8,128)(2,1)S(1)} %get-tuple-element.34), channel_id=1, source_target_pairs={{4,0},{8,4},{12,8},{16,12},{20,16},{24,20},{28,24},{32,28},{36,32}... | collective-permute-start | bytes 294920 | tf_op jit(solution)/shard_map/ppermute | solution.py:329
  109.0 3.5 %collective-permute-start.10 = (bf16[128,384]{1,0:T(8,128)(2,1)S(1)}, bf16[128,384]{1,0:T(8,128)(2,1)S(1)}, u32[]{:S(2)}, u32[]{:S(2)}) collective-permute-start(bf16[128,384]{1,0:T(8,128)(2,1)S(1)} %get-tuple-element.35), channel_id=1, source_target_pairs={{0,4},{4,8},{8,12},{12,16},{16,20},{20,24},{24,28},{28,32},{32,36}... | collective-permute-start | bytes 294920 | tf_op jit(solution)/shard_map/ppermute | solution.py:328
  112.5 2.1 %shard_map.134 = (bf16[256,256]{1,0:T(8,128)(2,1)S(1)}, f32[256,4]{1,0:T(8,128)S(1)}) custom-call(f32[4]{0:T(128)S(1)} %copy-done.3, bf16[512,256]{1,0:T(8,128)(2,1)S(1)} %get-tuple-element.21.query_ref, bf16[512,384]{1,0:T(8,128)(2,1)S(1)} %get-tuple-element.22.kvc_ref), custom_call_target="tpu_custom_call" | custom-call | flops 2013265920 | bytes 2000000 | tf_op jit(solution)/shard_map/pallas_call | solution.py:225
  114.6 2.9 %shard_map.135 = (bf16[128,2048]{1,0:T(8,128)(2,1)S(1)}, bf16[512,512]{1,0:T(8,128)(2,1)S(1)}, f32[256,4]{1,0:T(8,128)S(1)}) custom-call(f32[4]{0:T(128)S(1)} %copy-done.3, bf16[512,256]{1,0:T(8,128)(2,1)S(1)} %get-tuple-element.21.query_ref, bf16[512,384]{1,0:T(8,128)(2,1)S(1)} %get-tuple-element.22.kvc_ref, ...), custom_call_target="tpu_custom_call" | custom-call | flops 1073741824 | bytes 8000000 | tf_op jit(solution)/shard_map/pallas_call | solution.py:308
  117.5 2.3 %shard_map.137 = (bf16[128,2048]{1,0:T(8,128)(2,1)}, bf16[128,2048]{1,0:T(8,128)(2,1)}) custom-call(bf16[512,512]{1,0:T(8,128)(2,1)S(1)} %get-tuple-element.26.both_ref, bf16[2048,512]{1,0:T(8,128)(2,1)S(1)} %get-tuple-element.25.out_rows_ref), custom_call_target="tpu_custom_call" | custom-call | flops 536870912 | bytes 3000000 | tf_op jit(solution)/shard_map/pallas_call | solution.py:295
  119.8 2.6 %collective-permute-start.13 = (bf16[128,2048]{1,0:T(8,128)(2,1)}, bf16[128,2048]{1,0:T(8,128)(2,1)}, u32[]{:S(2)}, u32[]{:S(2)}) collective-permute-start(bf16[128,2048]{1,0:T(8,128)(2,1)} %get-tuple-element.28), channel_id=1, source_target_pairs={{3,0},{0,1},{1,2},{2,3},{7,4},{4,5},{5,6},{6,7},{11,8},{8,9},{9,10... | collective-permute-start | bytes 1572872 | tf_op jit(solution)/shard_map/ppermute | solution.py:33
  122.4 4.6 %collective-permute-start.14 = (bf16[128,2048]{1,0:T(8,128)(2,1)}, bf16[128,2048]{1,0:T(8,128)(2,1)}, u32[]{:S(2)}, u32[]{:S(2)}) collective-permute-start(bf16[128,2048]{1,0:T(8,128)(2,1)} %get-tuple-element.29), channel_id=1, source_target_pairs={{1,0},{2,1},{3,2},{0,3},{5,4},{6,5},{7,6},{4,7},{9,8},{10,9},{11,1... | collective-permute-start | bytes 1572872 | tf_op jit(solution)/shard_map/ppermute | solution.py:33
  126.9 3.1 %collective-permute-start.12 = (bf16[128,2048]{1,0:T(8,128)(2,1)S(1)}, bf16[128,2048]{1,0:T(8,128)(2,1)}, u32[]{:S(2)}, u32[]{:S(2)}) collective-permute-start(bf16[128,2048]{1,0:T(8,128)(2,1)S(1)} %get-tuple-element.27), channel_id=1, source_target_pairs={{2,0},{3,1},{0,2},{1,3},{6,4},{7,5},{4,6},{5,7},{10,8},{11,9},{8,1... | collective-permute-start | bytes 1572872 | tf_op jit(solution)/shard_map/ppermute | solution.py:33
  130.3 0.8 shard_map.136
  131.1 0.6 maximum_bitcast_fusion
  131.7 4.9 %collective-permute-done.13 = bf16[128,2048]{1,0:T(8,128)(2,1)} collective-permute-done((bf16[128,2048]{1,0:T(8,128)(2,1)}, bf16[128,2048]{1,0:T(8,128)(2,1)}, u32[]{:S(2)}, u32[]{:S(2)}) %collective-permute-start.13) | collective-permute-done | bytes 524320 | tf_op jit(solution)/shard_map/ppermute | solution.py:33
  136.6 13.0 %collective-permute-done.14 = bf16[128,2048]{1,0:T(8,128)(2,1)} collective-permute-done((bf16[128,2048]{1,0:T(8,128)(2,1)}, bf16[128,2048]{1,0:T(8,128)(2,1)}, u32[]{:S(2)}, u32[]{:S(2)}) %collective-permute-start.14) | collective-permute-done | bytes 524320 | tf_op jit(solution)/shard_map/ppermute | solution.py:33
  149.6 2.5 %add_convert_fusion = bf16[128,2048]{1,0:T(8,128)(2,1)} fusion(bf16[128,2048]{1,0:T(8,128)(2,1)} %collective-permute-done.14, bf16[128,2048]{1,0:T(8,128)(2,1)} %collective-permute-done.13, bf16[128,2048]{1,0:T(8,128)(2,1)} %collective-permute-done.12, bf16[128,2048]{1,0:T(8,128)(2,1)S(1)} %shard_map.136), kind=kLoop, calls=%fused_computation | loop fusion | flops 2097152 | bytes 2621440 | tf_op jit(solution)/shard_map/convert_element_type | solution.py:394
  (31 shorter events, 0.4 us)
Async XLA Ops:
  36.9 37.0 %collective-permute-start.5 = (bf16[16,16,1664]{2,1,0:T(8,128)(2,1)S(1)}, bf16[16,16,1664]{2,1,0:T(8,128)(2,1)S(1)}, u32[]{:S(2)}, u32[]{:S(2)}) collective-permute-start(bf16[16,16,1664]{2,1,0:T(8,128)(2,1)S(1)} %bitcast.6), channel_id=1, source_target_pairs={{24,0},{0,8},{8,16},{16,24},{25,1},{1,9},{9,17},{17,25},{26,2},{2,... | collective-permute-start | bytes 2555912 | tf_op jit(solution)/shard_map/ppermute | solution.py:33
  40.0 35.8 %collective-permute-start.4 = (bf16[16,16,1664]{2,1,0:T(8,128)(2,1)S(1)}, bf16[16,16,1664]{2,1,0:T(8,128)(2,1)S(1)}, u32[]{:S(2)}, u32[]{:S(2)}) collective-permute-start(bf16[16,16,1664]{2,1,0:T(8,128)(2,1)S(1)} %bitcast.7), channel_id=1, source_target_pairs={{16,0},{24,8},{0,16},{8,24},{17,1},{25,9},{1,17},{9,25},{18,2},{26... | collective-permute-start | bytes 2555912 | tf_op jit(solution)/shard_map/ppermute | solution.py:33
  44.4 38.1 %collective-permute-start.3 = (bf16[16,16,1664]{2,1,0:T(8,128)(2,1)S(1)}, bf16[16,16,1664]{2,1,0:T(8,128)(2,1)S(1)}, u32[]{:S(2)}, u32[]{:S(2)}) collective-permute-start(bf16[16,16,1664]{2,1,0:T(8,128)(2,1)S(1)} %bitcast.8), channel_id=1, source_target_pairs={{8,0},{16,8},{24,16},{0,24},{9,1},{17,9},{25,17},{1,25},{10,2},{18... | collective-permute-start | bytes 2555912 | tf_op jit(solution)/shard_map/ppermute | solution.py:33
  47.5 11.7 %collective-permute-start.2 = (bf16[512,512]{1,0:T(8,128)(2,1)}, bf16[512,512]{1,0:T(8,128)(2,1)S(1)}, u32[]{:S(2)}, u32[]{:S(2)}) collective-permute-start(bf16[512,512]{1,0:T(8,128)(2,1)} %tokens_ref.1), channel_id=1, source_target_pairs={{3,0},{0,1},{1,2},{2,3},{7,4},{4,5},{5,6},{6,7},{11,8},{8,9},{9,10... | collective-permute-start | bytes 1572872 | tf_op jit(solution)/shard_map/ppermute | solution.py:33
  50.7 33.8 %collective-permute-start.1 = (bf16[512,512]{1,0:T(8,128)(2,1)}, bf16[512,512]{1,0:T(8,128)(2,1)S(1)}, u32[]{:S(2)}, u32[]{:S(2)}) collective-permute-start(bf16[512,512]{1,0:T(8,128)(2,1)} %tokens_ref.1), channel_id=1, source_target_pairs={{2,0},{3,1},{0,2},{1,3},{6,4},{7,5},{4,6},{5,7},{10,8},{11,9},{8,1... | collective-permute-start | bytes 1572872 | tf_op jit(solution)/shard_map/ppermute | solution.py:33
  59.2 42.5 %collective-permute-start.6 = (bf16[16,16,1664]{2,1,0:T(8,128)(2,1)S(1)}, bf16[16,16,1664]{2,1,0:T(8,128)(2,1)S(1)}, u32[]{:S(2)}, u32[]{:S(2)}) collective-permute-start(bf16[16,16,1664]{2,1,0:T(8,128)(2,1)S(1)} %bitcast.9), channel_id=1, source_target_pairs={{4,0},{0,4},{5,1},{1,5},{6,2},{2,6},{7,3},{3,7},{12,8},{8,12},{13,... | collective-permute-start | bytes 2555912 | tf_op jit(solution)/shard_map/ppermute | solution.py:33
  73.9 27.8 %collective-permute-start.9 = (bf16[16,16,1664]{2,1,0:T(8,128)(2,1)S(1)}, bf16[16,16,1664]{2,1,0:T(8,128)(2,1)S(1)}, u32[]{:S(2)}, u32[]{:S(2)}) collective-permute-start(bf16[16,16,1664]{2,1,0:T(8,128)(2,1)S(1)} %collective-permute-done.5.refs_6_), channel_id=1, source_target_pairs={{4,0},{0,4},{5,1},{1,5},{6,2},{2,6},{7,3},{3,7},{12,8},{8,12},{13,... | collective-permute-start | bytes 2555912 | tf_op jit(solution)/shard_map/ppermute | solution.py:33
  75.8 25.8 %collective-permute-start.8 = (bf16[16,16,1664]{2,1,0:T(8,128)(2,1)S(1)}, bf16[16,16,1664]{2,1,0:T(8,128)(2,1)S(1)}, u32[]{:S(2)}, u32[]{:S(2)}) collective-permute-start(bf16[16,16,1664]{2,1,0:T(8,128)(2,1)S(1)} %collective-permute-done.4.refs_5_), channel_id=1, source_target_pairs={{4,0},{0,4},{5,1},{1,5},{6,2},{2,6},{7,3},{3,7},{12,8},{8,12},{13,... | collective-permute-start | bytes 2555912 | tf_op jit(solution)/shard_map/ppermute | solution.py:33
  82.5 19.1 %collective-permute-start.7 = (bf16[16,16,1664]{2,1,0:T(8,128)(2,1)S(1)}, bf16[16,16,1664]{2,1,0:T(8,128)(2,1)S(1)}, u32[]{:S(2)}, u32[]{:S(2)}) collective-permute-start(bf16[16,16,1664]{2,1,0:T(8,128)(2,1)S(1)} %collective-permute-done.3.refs_4_), channel_id=1, source_target_pairs={{4,0},{0,4},{5,1},{1,5},{6,2},{2,6},{7,3},{3,7},{12,8},{8,12},{13,... | collective-permute-start | bytes 2555912 | tf_op jit(solution)/shard_map/ppermute | solution.py:33
  84.5 15.7 %collective-permute-start = (bf16[512,512]{1,0:T(8,128)(2,1)}, bf16[512,512]{1,0:T(8,128)(2,1)S(1)}, u32[]{:S(2)}, u32[]{:S(2)}) collective-permute-start(bf16[512,512]{1,0:T(8,128)(2,1)} %tokens_ref.1), channel_id=1, source_target_pairs={{1,0},{2,1},{3,2},{0,3},{5,4},{6,5},{7,6},{4,7},{9,8},{10,9},{11,1... | collective-permute-start | bytes 1572872 | tf_op jit(solution)/shard_map/ppermute | solution.py:33
  89.1 1.1 copy-start
  90.2 0.7 copy-start.1
  101.6 10.9 %copy-start.3 = (f32[4]{0:T(128)S(1)}, f32[4]{0:T(128)}, u32[]{:S(2)}) copy-start(f32[4]{0:T(128)} %sink_ref.3) | copy-start | bytes 52
  105.7 8.9 %collective-permute-start.11 = (bf16[128,384]{1,0:T(8,128)(2,1)S(1)}, bf16[128,384]{1,0:T(8,128)(2,1)S(1)}, u32[]{:S(2)}, u32[]{:S(2)}) collective-permute-start(bf16[128,384]{1,0:T(8,128)(2,1)S(1)} %get-tuple-element.34), channel_id=1, source_target_pairs={{4,0},{8,4},{12,8},{16,12},{20,16},{24,20},{28,24},{32,28},{36,32}... | collective-permute-start | bytes 294920 | tf_op jit(solution)/shard_map/ppermute | solution.py:329
  109.0 5.6 %collective-permute-start.10 = (bf16[128,384]{1,0:T(8,128)(2,1)S(1)}, bf16[128,384]{1,0:T(8,128)(2,1)S(1)}, u32[]{:S(2)}, u32[]{:S(2)}) collective-permute-start(bf16[128,384]{1,0:T(8,128)(2,1)S(1)} %get-tuple-element.35), channel_id=1, source_target_pairs={{0,4},{4,8},{8,12},{12,16},{16,20},{20,24},{24,28},{28,32},{32,36}... | collective-permute-start | bytes 294920 | tf_op jit(solution)/shard_map/ppermute | solution.py:328
  112.5 2.1 %copy-start.2 = (f32[3,256]{1,0:T(4,128)S(1)}, f32[3,256]{1,0:T(4,128)}, u32[]{:S(2)}) copy-start(f32[3,256]{1,0:T(4,128)} %taps_ref.1) | copy-start | bytes 9220
  119.8 16.8 %collective-permute-start.13 = (bf16[128,2048]{1,0:T(8,128)(2,1)}, bf16[128,2048]{1,0:T(8,128)(2,1)}, u32[]{:S(2)}, u32[]{:S(2)}) collective-permute-start(bf16[128,2048]{1,0:T(8,128)(2,1)} %get-tuple-element.28), channel_id=1, source_target_pairs={{3,0},{0,1},{1,2},{2,3},{7,4},{4,5},{5,6},{6,7},{11,8},{8,9},{9,10... | collective-permute-start | bytes 1572872 | tf_op jit(solution)/shard_map/ppermute | solution.py:33
  122.4 27.2 %collective-permute-start.14 = (bf16[128,2048]{1,0:T(8,128)(2,1)}, bf16[128,2048]{1,0:T(8,128)(2,1)}, u32[]{:S(2)}, u32[]{:S(2)}) collective-permute-start(bf16[128,2048]{1,0:T(8,128)(2,1)} %get-tuple-element.29), channel_id=1, source_target_pairs={{1,0},{2,1},{3,2},{0,3},{5,4},{6,5},{7,6},{4,7},{9,8},{10,9},{11,1... | collective-permute-start | bytes 1572872 | tf_op jit(solution)/shard_map/ppermute | solution.py:33
  126.9 22.7 %collective-permute-start.12 = (bf16[128,2048]{1,0:T(8,128)(2,1)S(1)}, bf16[128,2048]{1,0:T(8,128)(2,1)}, u32[]{:S(2)}, u32[]{:S(2)}) collective-permute-start(bf16[128,2048]{1,0:T(8,128)(2,1)S(1)} %get-tuple-element.27), channel_id=1, source_target_pairs={{2,0},{3,1},{0,2},{1,3},{6,4},{7,5},{4,6},{5,7},{10,8},{11,9},{8,1... | collective-permute-start | bytes 1572872 | tf_op jit(solution)/shard_map/ppermute | solution.py:33
